TPU v7x, 32 devices: a whole 2x2x4 slice. The times are simulated.
32 devices in a mesh: fs: 8 (over z, x), tp: 4 (over y, core).
Axes of the slice: x: 2, y: 2, z: 4, core: 2. Of those that a mesh axis runs over, the one named last changes fastest.
Arguments:
- tokens: bfloat16 [16, 384, 2048], P('fs', None, 'tp'), may hold values from -20 to 20
- first_gain: float32 [2048], replicated, may hold values from 0.1 to 1.9
- first_gate: bfloat16 [2048, 5120], P('fs', 'tp'), may hold values from -0.125 to 0.125
- first_up: bfloat16 [2048, 5120], P('fs', 'tp'), may hold values from -0.125 to 0.125
- first_down: bfloat16 [5120, 2048], P('tp', 'fs'), may hold values from -0.078125 to 0.078125
- mixer_gain: float32 [2048], replicated, may hold values from 0.1 to 1.9
- conv_input: bfloat16 [2048, 1024], P('fs', 'tp'), may hold values from -0.125 to 0.125
- outer_gate: bfloat16 [2048, 1024], P('fs', 'tp'), may hold values from -0.125 to 0.125
- inner_gate: bfloat16 [2048, 1024], P('fs', 'tp'), may hold values from -0.125 to 0.125
- conv_taps: float32 [3, 1024], P(None, 'tp'), may hold values from -3.5 to 3.5
- mixer_out: bfloat16 [1024, 2048], P('tp', 'fs'), may hold values from -0.1875 to 0.1875
- second_gain: float32 [2048], replicated, may hold values from 0.1 to 1.9
- second_gate: bfloat16 [2048, 5120], P('fs', 'tp'), may hold values from -0.125 to 0.125
- second_up: bfloat16 [2048, 5120], P('fs', 'tp'), may hold values from -0.125 to 0.125
- second_down: bfloat16 [5120, 2048], P('tp', 'fs'), may hold values from -0.078125 to 0.078125
Outputs:
- layer_out: bfloat16 [16, 384, 2048], P('fs', None, 'tp')
All inputs are finite; a program needn't handle non-finite values.
Results may differ from a plain program's by a relative error of at most 0.015.
Values may be sent and summed in bfloat16 or wider, within the bound.
A program may use at most 64 MiB of HBM per device.

v0:
```python
import jax
import jax.numpy as jnp
from jax import lax
from jax.sharding import PartitionSpec as P

epsilon = 1e-05


def norm_rows(stream, gain):
    whole = lax.all_gather(stream, "tp", axis=1, tiled=True)
    values = whole.astype(jnp.float32)
    scale = lax.rsqrt(jnp.mean(values * values, axis=1, keepdims=True) + epsilon)
    return (values * scale * gain).astype(jnp.bfloat16)


def add_rows(gathered, piece):
    return jnp.dot(gathered, piece, preferred_element_type=jnp.float32)


def ffn_inputs(gathered, gate_weight, up_weight):
    empty = jnp.zeros((gathered.shape[0], gate_weight.shape[1]), jnp.float32)

    def add_single(total, piece, start):
        return add_rows(gathered, piece)

    gate = add_single(empty, lax.all_gather(gate_weight, "fs", axis=0, tiled=True), jnp.int32(0))
    upward = add_single(empty, lax.all_gather(up_weight, "fs", axis=0, tiled=True), jnp.int32(0))
    return (gate, upward)


def mixer_inputs(gathered, conv_input, outer_gate, inner_gate):
    empty = jnp.zeros((gathered.shape[0], conv_input.shape[1]), jnp.float32)

    def add_single(total, piece, start):
        return add_rows(gathered, piece)

    conv_values = add_single(
        empty, lax.all_gather(conv_input, "fs", axis=0, tiled=True), jnp.int32(0)
    )
    outer = add_single(empty, lax.all_gather(outer_gate, "fs", axis=0, tiled=True), jnp.int32(0))
    inner = add_single(empty, lax.all_gather(inner_gate, "fs", axis=0, tiled=True), jnp.int32(0))
    return (conv_values, outer, inner)


def project_down(hidden, weight):
    partial_sum = jnp.dot(
        hidden, lax.all_gather(weight, "fs", axis=1, tiled=True), preferred_element_type=jnp.float32
    )
    result = lax.psum_scatter(
        partial_sum.astype(jnp.bfloat16), "tp", scatter_dimension=1, tiled=True
    ).astype(jnp.float32)
    return result


def half_ffn(stream, gain, gate_weight, up_weight, down_weight):
    gathered = norm_rows(stream, gain)
    gate, upward = ffn_inputs(gathered, gate_weight, up_weight)
    hidden = (jax.nn.silu(gate) * upward).astype(jnp.bfloat16)
    branch = project_down(hidden, down_weight)
    return (stream.astype(jnp.float32) + 0.5 * branch).astype(jnp.bfloat16)


def conv_mixer(stream, seqs, gain, conv_input, outer_gate, inner_gate, conv_taps, mixer_out):
    gathered = norm_rows(stream, gain)
    conv_values, outer, inner = mixer_inputs(gathered, conv_input, outer_gate, inner_gate)
    gated_input = (inner * conv_values).reshape(seqs, -1, conv_values.shape[1])
    one_back = jnp.pad(gated_input, ((0, 0), (1, 0), (0, 0)))[:, :-1]
    two_back = jnp.pad(gated_input, ((0, 0), (2, 0), (0, 0)))[:, :-2]
    convolved = conv_taps[0] * two_back + conv_taps[1] * one_back + conv_taps[2] * gated_input
    mixed = (outer * convolved.reshape(conv_values.shape)).astype(jnp.bfloat16)
    branch = project_down(mixed, mixer_out)
    return (stream.astype(jnp.float32) + branch).astype(jnp.bfloat16)


def on_device(
    tokens,
    first_gain,
    first_gate,
    first_up,
    first_down,
    mixer_gain,
    conv_input,
    outer_gate,
    inner_gate,
    conv_taps,
    mixer_out,
    second_gain,
    second_gate,
    second_up,
    second_down,
):
    seqs, length, width = tokens.shape
    stream = tokens.reshape(seqs * length, width)
    stream = half_ffn(stream, first_gain, first_gate, first_up, first_down)
    stream = conv_mixer(
        stream, seqs, mixer_gain, conv_input, outer_gate, inner_gate, conv_taps, mixer_out
    )
    stream = half_ffn(stream, second_gain, second_gate, second_up, second_down)
    return stream.reshape(seqs, length, width)


def solution(mesh):
    in_specs = (
        P("fs", None, "tp"),
        P(),
        P("fs", "tp"),
        P("fs", "tp"),
        P("tp", "fs"),
        P(),
        P("fs", "tp"),
        P("fs", "tp"),
        P("fs", "tp"),
        P(None, "tp"),
        P("tp", "fs"),
        P(),
        P("fs", "tp"),
        P("fs", "tp"),
        P("tp", "fs"),
    )
    out_specs = P("fs", None, "tp")
    return jax.shard_map(
        on_device, mesh=mesh, in_specs=in_specs, out_specs=out_specs, check_vma=False
    )
```

profile of v0, /device:TPU:0, one launch (start us, length us, event | category | flops | bytes accessed | tf_op | source)
XLA Modules:
  0.0 947.5 jit_solution(4137865059658070734)
XLA Ops:
  6.5 0.7 all-gather.14.cloned.1.call-update
  7.3 0.0 all-gather.16.cloned.1.call-start
  7.3 0.7 all-gather.16.cloned.1.call-update
  8.0 0.0 all-gather.18.cloned.1.call-start
  8.1 0.7 all-gather.18.cloned.1.call-update
  8.7 0.0 all-gather.20.cloned.1.call-start
  8.8 0.5 all-gather.20.cloned.1.call-update
  9.3 0.0 reduce-scatter.4.cloned.1.call-start
  9.4 30.8 %all-gather.14.cloned.1.call-done = bf16[768,2048]{1,0:T(8,128)(2,1)} async-done(((bf16[768,512]{1,0:T(8,128)(2,1)}), bf16[768,2048]{1,0:T(8,128)(2,1)}) %all-gather.14.cloned.1.call-update) | async-done | bytes 3145744 | tf_op jit(solution)/shard_map/all_gather | solution.py:10
  40.2 2.6 fusion
  42.8 85.5 %all-gather.16.cloned.1.call-done = bf16[2048,1280]{1,0:T(8,128)(2,1)} async-done(((bf16[256,1280]{1,0:T(8,128)(2,1)}), bf16[2048,1280]{1,0:T(8,128)(2,1)}) %all-gather.16.cloned.1.call-update) | async-done | bytes 5242896 | tf_op jit(solution)/shard_map/all_gather | solution.py:26
  128.3 9.6 %fusion.18 = f32[768,1280]{1,0:T(8,128)} fusion(bf16[2048,1280]{1,0:T(8,128)(2,1)} %all-gather.16.cloned.1.call-done, bf16[768,2048]{1,0:T(8,128)(2,1)} %all-gather.14.cloned.1.call-done, f32[2048]{0:T(1024)S(1)} %copy-done.5, f32[768]{0:T(1024)S(1)} %add_rsqrt_fusion.2), kind=kOutput, calls=%fused_computation.29 | convolution fusion | flops 4032823296 | bytes 12332032 | tf_op jit(solution)/shard_map/dot_general | solution.py:17
  137.8 76.7 %all-gather.18.cloned.1.call-done = bf16[2048,1280]{1,0:T(8,128)(2,1)} async-done(((bf16[256,1280]{1,0:T(8,128)(2,1)}), bf16[2048,1280]{1,0:T(8,128)(2,1)}) %all-gather.18.cloned.1.call-update) | async-done | bytes 5242896 | tf_op jit(solution)/shard_map/all_gather | solution.py:27
  214.5 86.9 %all-gather.20.cloned.1.call-done = bf16[1280,2048]{1,0:T(8,128)(2,1)} async-done(((bf16[1280,256]{1,0:T(8,128)(2,1)}), bf16[1280,2048]{1,0:T(8,128)(2,1)}) %all-gather.20.cloned.1.call-update) | async-done | bytes 5242896 | tf_op jit(solution)/shard_map/all_gather | solution.py:47
  301.4 16.4 %convolution_convert_fusion.2 = bf16[768,2048]{1,0:T(8,128)(2,1)} fusion(bf16[1280,2048]{1,0:T(8,128)(2,1)} %all-gather.20.cloned.1.call-done, bf16[2048,1280]{1,0:T(8,128)(2,1)} %all-gather.18.cloned.1.call-done, f32[768,1280]{1,0:T(8,128)} %fusion.18, bf16[768,2048]{1,0:T(8,128)(2,1)S(1)} %copy-done.3, f32[2048]{0:T(1024)S(1)} %copy-done.5, ...), kind=kOutput, calls=%fused_computation.21 | convolution fusion | flops 8066826240 | bytes 20720640 | tf_op jit(solution)/shard_map/dot_general | solution.py:46
  317.8 0.0 reduce-scatter.4.cloned.1.call-update
  317.9 0.0 copy-start.6
  317.9 0.0 all-gather.22.cloned.1.call-start
  317.9 36.0 %reduce-scatter.4.cloned.1.call-done = bf16[768,512]{1,0:T(8,128)(2,1)} async-done(((bf16[768,2048]{1,0:T(8,128)(2,1)}), bf16[768,512]{1,0:T(8,128)(2,1)}) %reduce-scatter.4.cloned.1.call-update) | async-done | bytes 786448 | tf_op jit(solution)/shard_map/reduce_scatter | solution.py:49
  353.9 2.5 add_convert_fusion.2
  356.4 0.0 all-gather.22.cloned.1.call-update
  356.4 0.0 all-gather.26.cloned.1.call-start
  356.5 0.7 all-gather.26.cloned.1.call-update
  357.2 0.0 all-gather.28.cloned.1.call-start
  357.2 0.7 all-gather.28.cloned.1.call-update
  357.9 0.0 all-gather.24.cloned.1.call-start
  358.0 0.7 all-gather.24.cloned.1.call-update
  358.7 0.0 all-gather.30.cloned.1.call-start
  358.7 0.5 all-gather.30.cloned.1.call-update
  359.2 0.2 reduce-scatter.6.cloned.1.call-start
  359.5 25.6 %all-gather.22.cloned.1.call-done = bf16[768,2048]{1,0:T(8,128)(2,1)} async-done(((bf16[768,512]{1,0:T(8,128)(2,1)}), bf16[768,2048]{1,0:T(8,128)(2,1)}) %all-gather.22.cloned.1.call-update) | async-done | bytes 3145744 | tf_op jit(solution)/shard_map/all_gather | solution.py:10
  385.1 2.6 fusion.3
  387.7 39.8 %all-gather.26.cloned.1.call-done = bf16[2048,256]{1,0:T(8,128)(2,1)} async-done(((bf16[256,256]{1,0:T(8,128)(2,1)}), bf16[2048,256]{1,0:T(8,128)(2,1)}) %all-gather.26.cloned.1.call-update) | async-done | bytes 1048592 | tf_op jit(solution)/shard_map/all_gather | solution.py:41
  427.5 4.1 fusion.29
  431.6 37.0 %all-gather.28.cloned.1.call-done = bf16[2048,256]{1,0:T(8,128)(2,1)} async-done(((bf16[256,256]{1,0:T(8,128)(2,1)}), bf16[2048,256]{1,0:T(8,128)(2,1)}) %all-gather.28.cloned.1.call-update) | async-done | bytes 1048592 | tf_op jit(solution)/shard_map/all_gather | solution.py:38
  468.7 0.0 copy-done.2
  468.7 2.5 convolution_multiply_fusion.2
  471.1 0.2 fusion.24
  471.4 38.4 %all-gather.24.cloned.1.call-done = bf16[2048,256]{1,0:T(8,128)(2,1)} async-done(((bf16[256,256]{1,0:T(8,128)(2,1)}), bf16[2048,256]{1,0:T(8,128)(2,1)}) %all-gather.24.cloned.1.call-update) | async-done | bytes 1048592 | tf_op jit(solution)/shard_map/all_gather | solution.py:40
  509.8 40.0 %all-gather.30.cloned.1.call-done = bf16[256,2048]{1,0:T(8,128)(2,1)} async-done(((bf16[256,256]{1,0:T(8,128)(2,1)}), bf16[256,2048]{1,0:T(8,128)(2,1)}) %all-gather.30.cloned.1.call-update) | async-done | bytes 1048592 | tf_op jit(solution)/shard_map/all_gather | solution.py:47
  549.8 7.6 convolution_convert_fusion
  557.5 0.0 reduce-scatter.6.cloned.1.call-update
  557.5 0.0 copy-start.7
  557.5 0.0 all-gather.32.cloned.1.call-start
  557.5 36.8 %reduce-scatter.6.cloned.1.call-done = bf16[768,512]{1,0:T(8,128)(2,1)} async-done(((bf16[768,2048]{1,0:T(8,128)(2,1)}), bf16[768,512]{1,0:T(8,128)(2,1)}) %reduce-scatter.6.cloned.1.call-update) | async-done | bytes 786448 | tf_op jit(solution)/shard_map/reduce_scatter | solution.py:49
  594.4 2.2 add_convert_fusion.1
  596.6 0.0 all-gather.32.cloned.1.call-update
  596.6 0.0 all-gather.34.cloned.1.call-start
  596.7 0.7 all-gather.34.cloned.1.call-update
  597.4 0.0 all-gather.36.cloned.1.call-start
  597.4 0.5 all-gather.36.cloned.1.call-update
  598.0 0.0 all-gather.38.cloned.1.call-start
  598.0 0.5 all-gather.38.cloned.1.call-update
  598.5 0.3 reduce-scatter.8.cloned.1.call-start
  598.8 26.5 %all-gather.32.cloned.1.call-done = bf16[768,2048]{1,0:T(8,128)(2,1)} async-done(((bf16[768,512]{1,0:T(8,128)(2,1)}), bf16[768,2048]{1,0:T(8,128)(2,1)}) %all-gather.32.cloned.1.call-update) | async-done | bytes 3145744 | tf_op jit(solution)/shard_map/all_gather | solution.py:10
  625.3 2.6 fusion.6
  627.9 85.5 %all-gather.34.cloned.1.call-done = bf16[2048,1280]{1,0:T(8,128)(2,1)} async-done(((bf16[256,1280]{1,0:T(8,128)(2,1)}), bf16[2048,1280]{1,0:T(8,128)(2,1)}) %all-gather.34.cloned.1.call-update) | async-done | bytes 5242896 | tf_op jit(solution)/shard_map/all_gather | solution.py:26
  713.4 9.6 %fusion.13 = f32[768,1280]{1,0:T(8,128)} fusion(bf16[2048,1280]{1,0:T(8,128)(2,1)} %all-gather.34.cloned.1.call-done, bf16[768,2048]{1,0:T(8,128)(2,1)} %all-gather.32.cloned.1.call-done, f32[2048]{0:T(1024)S(1)} %copy-done.7, f32[768]{0:T(1024)S(1)} %add_rsqrt_fusion), kind=kOutput, calls=%fused_computation.28 | convolution fusion | flops 4032823296 | bytes 12332032 | tf_op jit(solution)/shard_map/dot_general | solution.py:17
  723.0 76.5 %all-gather.36.cloned.1.call-done = bf16[2048,1280]{1,0:T(8,128)(2,1)} async-done(((bf16[256,1280]{1,0:T(8,128)(2,1)}), bf16[2048,1280]{1,0:T(8,128)(2,1)}) %all-gather.36.cloned.1.call-update) | async-done | bytes 5242896 | tf_op jit(solution)/shard_map/all_gather | solution.py:27
  799.5 86.9 %all-gather.38.cloned.1.call-done = bf16[1280,2048]{1,0:T(8,128)(2,1)} async-done(((bf16[1280,256]{1,0:T(8,128)(2,1)}), bf16[1280,2048]{1,0:T(8,128)(2,1)}) %all-gather.38.cloned.1.call-update) | async-done | bytes 5242896 | tf_op jit(solution)/shard_map/all_gather | solution.py:47
  886.4 16.2 %convolution_convert_fusion.1 = bf16[768,2048]{1,0:T(8,128)(2,1)} fusion(bf16[1280,2048]{1,0:T(8,128)(2,1)} %all-gather.38.cloned.1.call-done, bf16[2048,1280]{1,0:T(8,128)(2,1)} %all-gather.36.cloned.1.call-done, f32[768,1280]{1,0:T(8,128)} %fusion.13, bf16[768,2048]{1,0:T(8,128)(2,1)} %all-gather.32.cloned.1.call-done, f32[2048]{0:T(1024)S(1)} %copy-done.7, ...), kind=kOutput, calls=%fused_computation.20 | convolution fusion | flops 8066826240 | bytes 20720640 | tf_op jit(solution)/shard_map/dot_general | solution.py:46
  902.6 0.0 reduce-scatter.8.cloned.1.call-update
  902.6 36.1 %reduce-scatter.8.cloned.1.call-done = bf16[768,512]{1,0:T(8,128)(2,1)} async-done(((bf16[768,2048]{1,0:T(8,128)(2,1)}), bf16[768,512]{1,0:T(8,128)(2,1)}) %reduce-scatter.8.cloned.1.call-update) | async-done | bytes 786448 | tf_op jit(solution)/shard_map/reduce_scatter | solution.py:49
  938.7 2.2 add_convert_fusion
  (18 shorter events, 0.1 us)
Async XLA Ops:
  6.5 121.7 %copy-start.5 = (f32[2048]{0:T(1024)S(1)}, f32[2048]{0:T(1024)}, u32[]{:S(2)}) copy-start(f32[2048]{0:T(1024)} %param.16) | copy-start | bytes 24580
  6.5 33.6 %all-gather.14.cloned.1.call-start = ((), (), s32[]{:S(2)}) async-start(), calls=%async_computation.3 | async-start | bytes 3932160 | tf_op jit(solution)/shard_map/all_gather | solution.py:10
  7.3 121.0 %all-gather.16.cloned.1.call-start = ((), (), s32[]{:S(2)}) async-start(), calls=%async_computation.4 | async-start | bytes 5898240 | tf_op jit(solution)/shard_map/all_gather | solution.py:26
  8.0 206.5 %all-gather.18.cloned.1.call-start = ((), (), s32[]{:S(2)}) async-start(), calls=%async_computation.5 | async-start | bytes 5898240 | tf_op jit(solution)/shard_map/all_gather | solution.py:27
  8.7 292.7 %all-gather.20.cloned.1.call-start = ((), (), s32[]{:S(2)}) async-start(), calls=%async_computation.6 | async-start | bytes 5898240 | tf_op jit(solution)/shard_map/all_gather | solution.py:47
  9.3 344.6 %reduce-scatter.4.cloned.1.call-start = ((), (), s32[]{:S(2)}) async-start(), calls=%async_computation.7 | async-start | bytes 3932160 | tf_op jit(solution)/shard_map/reduce_scatter | solution.py:49
  42.7 258.7 %copy-start.3 = (bf16[768,2048]{1,0:T(8,128)(2,1)S(1)}, bf16[768,2048]{1,0:T(8,128)(2,1)}, u32[]{:S(2)}) copy-start(bf16[768,2048]{1,0:T(8,128)(2,1)} %all-gather.14.cloned.1.call-done) | copy-start | bytes 9437188
  317.8 41.6 %copy-start.4 = (f32[3,256]{1,0:T(4,128)S(1)}, f32[3,256]{1,0:T(4,128)}, u32[]{:S(2)}) copy-start(f32[3,256]{1,0:T(4,128)} %param.24) | copy-start | bytes 9220
  317.9 109.6 %copy-start.6 = (f32[2048]{0:T(1024)S(1)}, f32[2048]{0:T(1024)}, u32[]{:S(2)}) copy-start(f32[2048]{0:T(1024)} %param.20) | copy-start | bytes 24580
  317.9 67.2 %all-gather.22.cloned.1.call-start = ((), (), s32[]{:S(2)}) async-start(), calls=%async_computation.8 | async-start | bytes 3932160 | tf_op jit(solution)/shard_map/all_gather | solution.py:10
  356.4 71.1 %all-gather.26.cloned.1.call-start = ((), (), s32[]{:S(2)}) async-start(), calls=%async_computation.10 | async-start | bytes 1179648 | tf_op jit(solution)/shard_map/all_gather | solution.py:41
  357.2 111.5 %all-gather.28.cloned.1.call-start = ((), (), s32[]{:S(2)}) async-start(), calls=%async_computation.11 | async-start | bytes 1179648 | tf_op jit(solution)/shard_map/all_gather | solution.py:38
  357.9 151.9 %all-gather.24.cloned.1.call-start = ((), (), s32[]{:S(2)}) async-start(), calls=%async_computation.9 | async-start | bytes 1179648 | tf_op jit(solution)/shard_map/all_gather | solution.py:40
  358.7 191.2 %all-gather.30.cloned.1.call-start = ((), (), s32[]{:S(2)}) async-start(), calls=%async_computation.12 | async-start | bytes 1179648 | tf_op jit(solution)/shard_map/all_gather | solution.py:47
  359.2 235.1 %reduce-scatter.6.cloned.1.call-start = ((), (), s32[]{:S(2)}) async-start(), calls=%async_computation.13 | async-start | bytes 3932160 | tf_op jit(solution)/shard_map/reduce_scatter | solution.py:49
  387.7 81.0 %copy-start.2 = (bf16[768,2048]{1,0:T(8,128)(2,1)S(1)}, bf16[768,2048]{1,0:T(8,128)(2,1)}, u32[]{:S(2)}) copy-start(bf16[768,2048]{1,0:T(8,128)(2,1)} %all-gather.22.cloned.1.call-done) | copy-start | bytes 9437188
  549.8 44.5 %copy-start = (bf16[768,512]{1,0:T(8,128)(2,1)S(1)}, bf16[768,512]{1,0:T(8,128)(2,1)}, u32[]{:S(2)}) copy-start(bf16[768,512]{1,0:T(8,128)(2,1)} %add_convert_fusion.2) | copy-start | bytes 2359300
  557.5 155.9 %copy-start.7 = (f32[2048]{0:T(1024)S(1)}, f32[2048]{0:T(1024)}, u32[]{:S(2)}) copy-start(f32[2048]{0:T(1024)} %param.26) | copy-start | bytes 24580
  557.5 67.8 %all-gather.32.cloned.1.call-start = ((), (), s32[]{:S(2)}) async-start(), calls=%async_computation.14 | async-start | bytes 3932160 | tf_op jit(solution)/shard_map/all_gather | solution.py:10
  596.6 116.8 %all-gather.34.cloned.1.call-start = ((), (), s32[]{:S(2)}) async-start(), calls=%async_computation.15 | async-start | bytes 5898240 | tf_op jit(solution)/shard_map/all_gather | solution.py:26
  597.4 202.1 %all-gather.36.cloned.1.call-start = ((), (), s32[]{:S(2)}) async-start(), calls=%async_computation.16 | async-start | bytes 5898240 | tf_op jit(solution)/shard_map/all_gather | solution.py:27
  598.0 288.4 %all-gather.38.cloned.1.call-start = ((), (), s32[]{:S(2)}) async-start(), calls=%async_computation.17 | async-start | bytes 5898240 | tf_op jit(solution)/shard_map/all_gather | solution.py:47
  598.5 340.2 %reduce-scatter.8.cloned.1.call-start = ((), (), s32[]{:S(2)}) async-start(), calls=%async_computation.18 | async-start | bytes 3932160 | tf_op jit(solution)/shard_map/reduce_scatter | solution.py:49
  723.0 215.7 %copy-start.1 = (bf16[768,512]{1,0:T(8,128)(2,1)S(1)}, bf16[768,512]{1,0:T(8,128)(2,1)}, u32[]{:S(2)}) copy-start(bf16[768,512]{1,0:T(8,128)(2,1)} %add_convert_fusion.1) | copy-start | bytes 2359300
Sparse Core Ops, SparseCore 0:
  8.9 31.2 all-gather.13
  42.3 85.8 all-gather.15
  130.4 84.0 all-gather.17
  216.4 84.9 all-gather.19
  318.0 35.8 reduce-scatter.3
  356.5 28.4 all-gather.21
  387.2 40.2 all-gather.25
  429.6 38.9 all-gather.27
  470.8 38.9 all-gather.23
  511.7 38.0 all-gather.29
  557.6 36.7 reduce-scatter.5
  596.7 28.5 all-gather.31
  627.5 85.8 all-gather.33
  715.4 84.0 all-gather.35
  801.4 84.9 all-gather.37
  902.8 35.8 reduce-scatter.7
where the time goes:
time: 948 us; the launch traced here: 947 us
  waiting for transfers between devices  852 us (90%)
  matrix products  66 us (7%)
  other arithmetic  14.9 us (2%)
  between operations  13.4 us (1%)
    all_gather x3, waiting for transfers between devices, project_down(): lax.all_gather(weight, 'fs', axis=1, tiled=True)  214 us
    all_gather x2, waiting for transfers between devices, ffn_inputs(): lax.all_gather(gate_weight, 'fs', axis=0, tiled=True)  171 us
    all_gather x2, waiting for transfers between devices, ffn_inputs(): lax.all_gather(up_weight, 'fs', axis=0, tiled=True)  153 us
    reduce_scatter x3, waiting for transfers between devices, project_down(): lax.psum_scatter(partial_sum.astype(jnp.bfloat16), 'tp', scatter_dimensio...  109 us
    all_gather x3, waiting for transfers between devices, norm_rows(): whole = lax.all_gather(stream, 'tp', axis=1, tiled=True)  82.9 us
    dot_general x3, matrix products, project_down(): jnp.dot(hidden, lax.all_gather(weight, 'fs', axis=1, tiled=True), preferr...  40.2 us
    all_gather x1, waiting for transfers between devices, mixer_inputs(): lax.all_gather(inner_gate, 'fs', axis=0, tiled=True)  39.8 us
    all_gather x1, waiting for transfers between devices, mixer_inputs(): lax.all_gather(outer_gate, 'fs', axis=0, tiled=True)  38.4 us
  transfers between devices with their start and end apart: 16, of which 16 were waited for; matrix products, arithmetic and copies ran while one was open for 4% of the time, Pallas kernels for 0%

commit v1 on v0

--- a/solution.py
+++ b/solution.py
@@ -7,7 +7,12 @@
 
 
 def norm_rows(stream, gain):
-    whole = lax.all_gather(stream, "tp", axis=1, tiled=True)
+    ring = [stream]
+    for hop in range(3):
+        ring.append(lax.ppermute(ring[-1], "tp", [(dev, (dev + 1) % 4) for dev in range(4)]))
+    whole = jnp.roll(
+        jnp.concatenate(ring[::-1], axis=1), (lax.axis_index("tp") + 1) * ring[0].shape[1], axis=1
+    )
     values = whole.astype(jnp.float32)
     scale = lax.rsqrt(jnp.mean(values * values, axis=1, keepdims=True) + epsilon)
     return (values * scale * gain).astype(jnp.bfloat16)

time: 948 us -> 855 us (0.902)
  waiting for transfers between devices: 852 us -> 742 us
  other arithmetic: 14.9 us -> 32.4 us
    ppermute x0 -> x9, waiting for transfers between devices: none -> 102 us  [norm_rows(): lax.ppermute(ring[-1], 'tp', [(dev, (dev + 1) % 4) for dev in range(4)])]
    all_gather x2, waiting for transfers between devices: 171 us -> 88 us  [ffn_inputs(): lax.all_gather(gate_weight, 'fs', axis=0, tiled=True)]
    all_gather x3 -> x0, waiting for transfers between devices: 82.9 us -> none  [norm_rows(): whole = lax.all_gather(stream, 'tp', axis=1, tiled=True)]
    all_gather x1, waiting for transfers between devices: 37 us -> 0.01 us  [mixer_inputs(): lax.all_gather(conv_input, 'fs', axis=0, tiled=True)]
    reduce_sum x3, other arithmetic: 7.71 us -> 27 us  [norm_rows(): jnp.mean(values * values, axis=1, keepdims=True) + epsilon]
  transfers between devices with their start and end apart: 16 -> 22, of which waited for: 16 -> 21; matrix products, arithmetic and copies ran while one was open for 4% -> 6% of each run, Pallas kernels for 0% -> 0%
where the time goes in v1:
time: 855 us
  waiting for transfers between devices  742 us (87%)
  matrix products  64.8 us (8%)
  other arithmetic  32.4 us (4%)
  between operations  13.4 us (2%)
    all_gather x3, waiting for transfers between devices, project_down(): lax.all_gather(weight, 'fs', axis=1, tiled=True)  214 us
    all_gather x2, waiting for transfers between devices, ffn_inputs(): lax.all_gather(up_weight, 'fs', axis=0, tiled=True)  154 us
    reduce_scatter x3, waiting for transfers between devices, project_down(): lax.psum_scatter(partial_sum.astype(jnp.bfloat16), 'tp', scatter_dimensio...  106 us
    ppermute x9, waiting for transfers between devices, norm_rows(): lax.ppermute(ring[-1], 'tp', [(dev, (dev + 1) % 4) for dev in range(4)])  102 us
    all_gather x2, waiting for transfers between devices, ffn_inputs(): lax.all_gather(gate_weight, 'fs', axis=0, tiled=True)  88 us
    dot_general x3, matrix products, project_down(): jnp.dot(hidden, lax.all_gather(weight, 'fs', axis=1, tiled=True), preferr...  40.1 us
    all_gather x1, waiting for transfers between devices, mixer_inputs(): lax.all_gather(outer_gate, 'fs', axis=0, tiled=True)  37.7 us
    all_gather x1, waiting for transfers between devices, mixer_inputs(): lax.all_gather(inner_gate, 'fs', axis=0, tiled=True)  34.6 us
  transfers between devices with their start and end apart: 22, of which 21 were waited for; matrix products, arithmetic and copies ran while one was open for 6% of the time, Pallas kernels for 0%

profile of v1, /device:TPU:0, one launch (start us, length us, event | category | flops | bytes accessed | tf_op | source)
XLA Modules:
  0.0 855.2 jit_solution(7523875683802167748)
XLA Ops:
  6.5 0.7 all-gather.11.cloned.1.call-update
  7.3 0.0 all-gather.13.cloned.1.call-start
  7.3 0.7 all-gather.13.cloned.1.call-update
  8.0 0.0 all-gather.15.cloned.1.call-start
  8.1 0.7 all-gather.15.cloned.1.call-update
  8.7 0.0 reduce-scatter.4.cloned.1.call-start
  8.8 0.5 collective-permute-start
  9.3 11.8 %collective-permute-done = bf16[768,512]{1,0:T(8,128)(2,1)S(1)} collective-permute-done((bf16[768,512]{1,0:T(8,128)(2,1)}, bf16[768,512]{1,0:T(8,128)(2,1)S(1)}, u32[]{:S(2)}, u32[]{:S(2)}) %collective-permute-start) | collective-permute-done | bytes 786464 | tf_op jit(solution)/shard_map/ppermute | solution.py:12
  21.2 0.9 copy-done
  22.0 0.0 collective-permute-start.1
  22.1 11.4 %collective-permute-done.1 = bf16[768,512]{1,0:T(8,128)(2,1)S(1)} collective-permute-done((bf16[768,512]{1,0:T(8,128)(2,1)S(1)}, bf16[768,512]{1,0:T(8,128)(2,1)S(1)}, u32[]{:S(2)}, u32[]{:S(2)}) %collective-permute-start.1) | collective-permute-done | bytes 786464 | tf_op jit(solution)/shard_map/ppermute | solution.py:12
  33.5 0.9 copy-done.1
  34.3 10.6 %collective-permute-done.2 = bf16[768,512]{1,0:T(8,128)(2,1)} collective-permute-done((bf16[768,512]{1,0:T(8,128)(2,1)S(1)}, bf16[768,512]{1,0:T(8,128)(2,1)}, u32[]{:S(2)}, u32[]{:S(2)}) %collective-permute-start.2) | collective-permute-done | bytes 786464 | tf_op jit(solution)/shard_map/ppermute | solution.py:12
  45.0 7.9 fusion
  52.9 45.2 %all-gather.11.cloned.1.call-done = bf16[2048,1280]{1,0:T(8,128)(2,1)} async-done(((bf16[256,1280]{1,0:T(8,128)(2,1)}), bf16[2048,1280]{1,0:T(8,128)(2,1)}) %all-gather.11.cloned.1.call-update) | async-done | bytes 5242896 | tf_op jit(solution)/shard_map/all_gather | solution.py:31
  98.2 8.6 %fusion.39 = f32[768,1280]{1,0:T(8,128)} fusion(bf16[2048,1280]{1,0:T(8,128)(2,1)} %all-gather.11.cloned.1.call-done, bf16[768,2048]{1,0:T(8,128)(2,1)S(1)} %get-tuple-element.11, f32[2048]{0:T(1024)S(1)} %copy-done.3, f32[768]{0:T(1024)S(1)} %add_rsqrt_fusion.2), kind=kOutput, calls=%fused_computation.74 | convolution fusion | flops 4032823296 | bytes 12332032 | tf_op jit(solution)/shard_map/dot_general | solution.py:22
  106.8 77.6 %all-gather.13.cloned.1.call-done = bf16[2048,1280]{1,0:T(8,128)(2,1)} async-done(((bf16[256,1280]{1,0:T(8,128)(2,1)}), bf16[2048,1280]{1,0:T(8,128)(2,1)}) %all-gather.13.cloned.1.call-update) | async-done | bytes 5242896 | tf_op jit(solution)/shard_map/all_gather | solution.py:32
  184.4 87.0 %all-gather.15.cloned.1.call-done = bf16[1280,2048]{1,0:T(8,128)(2,1)} async-done(((bf16[1280,256]{1,0:T(8,128)(2,1)}), bf16[1280,2048]{1,0:T(8,128)(2,1)}) %all-gather.15.cloned.1.call-update) | async-done | bytes 5242896 | tf_op jit(solution)/shard_map/all_gather | solution.py:52
  271.5 16.4 %convolution_convert_fusion.2 = bf16[768,2048]{1,0:T(8,128)(2,1)} fusion(bf16[1280,2048]{1,0:T(8,128)(2,1)} %all-gather.15.cloned.1.call-done, bf16[2048,1280]{1,0:T(8,128)(2,1)} %all-gather.13.cloned.1.call-done, f32[768,1280]{1,0:T(8,128)} %fusion.39, bf16[768,2048]{1,0:T(8,128)(2,1)S(1)} %get-tuple-element.11, f32[2048]{0:T(1024)S(1)} %copy-done.3, ...), kind=kOutput, calls=%fused_computation.45 | convolution fusion | flops 8066826240 | bytes 20720640 | tf_op jit(solution)/shard_map/dot_general | solution.py:51
  287.9 0.0 all-gather.21.cloned.1.call-start
  288.0 0.5 all-gather.21.cloned.1.call-update
  288.5 0.0 all-gather.19.cloned.1.call-start
  288.5 0.5 all-gather.19.cloned.1.call-update
  289.1 0.0 all-gather.17.cloned.1.call-start
  289.1 34.8 %reduce-scatter.4.cloned.1.call-done = bf16[768,512]{1,0:T(8,128)(2,1)} async-done(((bf16[768,2048]{1,0:T(8,128)(2,1)}), bf16[768,512]{1,0:T(8,128)(2,1)}) %reduce-scatter.4.cloned.1.call-update) | async-done | bytes 786448 | tf_op jit(solution)/shard_map/reduce_scatter | solution.py:54
  324.0 1.6 add_convert_fusion.2
  325.6 0.1 collective-permute-start.3
  325.6 0.0 all-gather.17.cloned.1.call-update
  325.6 0.0 all-gather.23.cloned.1.call-start
  325.7 11.3 %collective-permute-done.3 = bf16[768,512]{1,0:T(8,128)(2,1)S(1)} collective-permute-done((bf16[768,512]{1,0:T(8,128)(2,1)S(1)}, bf16[768,512]{1,0:T(8,128)(2,1)S(1)}, u32[]{:S(2)}, u32[]{:S(2)}) %collective-permute-start.3) | collective-permute-done | bytes 786464 | tf_op jit(solution)/shard_map/ppermute | solution.py:12
  337.0 11.4 %collective-permute-done.4 = bf16[768,512]{1,0:T(8,128)(2,1)S(1)} collective-permute-done((bf16[768,512]{1,0:T(8,128)(2,1)S(1)}, bf16[768,512]{1,0:T(8,128)(2,1)S(1)}, u32[]{:S(2)}, u32[]{:S(2)}) %collective-permute-start.4) | collective-permute-done | bytes 786464 | tf_op jit(solution)/shard_map/ppermute | solution.py:12
  348.4 0.0 all-gather.23.cloned.1.call-update
  348.5 0.0 reduce-scatter.6.cloned.1.call-start
  348.5 11.3 %collective-permute-done.5 = bf16[768,512]{1,0:T(8,128)(2,1)S(1)} collective-permute-done((bf16[768,512]{1,0:T(8,128)(2,1)S(1)}, bf16[768,512]{1,0:T(8,128)(2,1)S(1)}, u32[]{:S(2)}, u32[]{:S(2)}) %collective-permute-start.5) | collective-permute-done | bytes 786464 | tf_op jit(solution)/shard_map/ppermute | solution.py:12
  359.9 9.5 %fusion.3 = (f32[768]{0:T(1024)S(1)}, bf16[768,2048]{1,0:T(8,128)(2,1)}) fusion(s32[]{:T(128)S(6)} %select_n.15, bf16[768,512]{1,0:T(8,128)(2,1)S(1)} %add_convert_fusion.2, bf16[768,512]{1,0:T(8,128)(2,1)S(1)} %collective-permute-done.3, bf16[768,512]{1,0:T(8,128)(2,1)S(1)} %collective-permute-done.4, bf16[768,512]{1,0:T(8,128)(2,1)S(1)} %collective-permute-done.5), kind=kLoop, calls=%fused_computation.9 | loop fusion | flops 29883648 | bytes 6294532 | tf_op jit(solution)/shard_map/reduce_sum | solution.py:17
  369.4 3.2 fusion.49
  372.6 34.6 %all-gather.19.cloned.1.call-done = bf16[2048,256]{1,0:T(8,128)(2,1)} async-done(((bf16[256,256]{1,0:T(8,128)(2,1)}), bf16[2048,256]{1,0:T(8,128)(2,1)}) %all-gather.19.cloned.1.call-update) | async-done | bytes 1048592 | tf_op jit(solution)/shard_map/all_gather | solution.py:46
  407.2 3.2 convolution_multiply_fusion.2
  410.4 0.2 fusion.45
  410.7 37.7 %all-gather.17.cloned.1.call-done = bf16[2048,256]{1,0:T(8,128)(2,1)} async-done(((bf16[256,256]{1,0:T(8,128)(2,1)}), bf16[2048,256]{1,0:T(8,128)(2,1)}) %all-gather.17.cloned.1.call-update) | async-done | bytes 1048592 | tf_op jit(solution)/shard_map/all_gather | solution.py:45
  448.4 40.2 %all-gather.23.cloned.1.call-done = bf16[256,2048]{1,0:T(8,128)(2,1)} async-done(((bf16[256,256]{1,0:T(8,128)(2,1)}), bf16[256,2048]{1,0:T(8,128)(2,1)}) %all-gather.23.cloned.1.call-update) | async-done | bytes 1048592 | tf_op jit(solution)/shard_map/all_gather | solution.py:52
  488.6 7.5 convolution_convert_fusion
  496.1 0.0 all-gather.25.cloned.1.call-start
  496.2 0.5 all-gather.25.cloned.1.call-update
  496.7 0.0 all-gather.27.cloned.1.call-start
  496.8 0.7 all-gather.27.cloned.1.call-update
  497.4 0.0 all-gather.29.cloned.1.call-start
  497.5 0.5 all-gather.29.cloned.1.call-update
  498.0 0.0 reduce-scatter.8.cloned.1.call-start
  498.1 34.9 %reduce-scatter.6.cloned.1.call-done = bf16[768,512]{1,0:T(8,128)(2,1)} async-done(((bf16[768,2048]{1,0:T(8,128)(2,1)}), bf16[768,512]{1,0:T(8,128)(2,1)}) %reduce-scatter.6.cloned.1.call-update) | async-done | bytes 786448 | tf_op jit(solution)/shard_map/reduce_scatter | solution.py:54
  533.0 1.3 add_convert_fusion.1
  534.3 0.1 collective-permute-start.6
  534.4 11.4 %collective-permute-done.6 = bf16[768,512]{1,0:T(8,128)(2,1)S(1)} collective-permute-done((bf16[768,512]{1,0:T(8,128)(2,1)S(1)}, bf16[768,512]{1,0:T(8,128)(2,1)S(1)}, u32[]{:S(2)}, u32[]{:S(2)}) %collective-permute-start.6) | collective-permute-done | bytes 786464 | tf_op jit(solution)/shard_map/ppermute | solution.py:12
  545.8 11.4 %collective-permute-done.7 = bf16[768,512]{1,0:T(8,128)(2,1)S(1)} collective-permute-done((bf16[768,512]{1,0:T(8,128)(2,1)S(1)}, bf16[768,512]{1,0:T(8,128)(2,1)S(1)}, u32[]{:S(2)}, u32[]{:S(2)}) %collective-permute-start.7) | collective-permute-done | bytes 786464 | tf_op jit(solution)/shard_map/ppermute | solution.py:12
  557.2 11.4 %collective-permute-done.8 = bf16[768,512]{1,0:T(8,128)(2,1)S(1)} collective-permute-done((bf16[768,512]{1,0:T(8,128)(2,1)S(1)}, bf16[768,512]{1,0:T(8,128)(2,1)S(1)}, u32[]{:S(2)}, u32[]{:S(2)}) %collective-permute-start.8) | collective-permute-done | bytes 786464 | tf_op jit(solution)/shard_map/ppermute | solution.py:12
  568.6 9.5 %fusion.6 = (f32[768]{0:T(1024)S(1)}, bf16[768,2048]{1,0:T(8,128)(2,1)}) fusion(s32[]{:T(128)S(6)} %select_n.15, bf16[768,512]{1,0:T(8,128)(2,1)S(1)} %add_convert_fusion.1, bf16[768,512]{1,0:T(8,128)(2,1)S(1)} %collective-permute-done.6, bf16[768,512]{1,0:T(8,128)(2,1)S(1)} %collective-permute-done.7, bf16[768,512]{1,0:T(8,128)(2,1)S(1)} %collective-permute-done.8), kind=kLoop, calls=%fused_computation.12 | loop fusion | flops 29883648 | bytes 6294532 | tf_op jit(solution)/shard_map/reduce_sum | solution.py:17
  578.2 42.8 %all-gather.25.cloned.1.call-done = bf16[2048,1280]{1,0:T(8,128)(2,1)} async-done(((bf16[256,1280]{1,0:T(8,128)(2,1)}), bf16[2048,1280]{1,0:T(8,128)(2,1)}) %all-gather.25.cloned.1.call-update) | async-done | bytes 5242896 | tf_op jit(solution)/shard_map/all_gather | solution.py:31
  621.0 9.6 %fusion.34 = f32[768,1280]{1,0:T(8,128)} fusion(bf16[2048,1280]{1,0:T(8,128)(2,1)} %all-gather.25.cloned.1.call-done, bf16[768,2048]{1,0:T(8,128)(2,1)} %get-tuple-element.7, f32[2048]{0:T(1024)S(1)} %copy-done.5, f32[768]{0:T(1024)S(1)} %add_rsqrt_fusion), kind=kOutput, calls=%fused_computation.73 | convolution fusion | flops 4032823296 | bytes 12332032 | tf_op jit(solution)/shard_map/dot_general | solution.py:22
  630.5 76.7 %all-gather.27.cloned.1.call-done = bf16[2048,1280]{1,0:T(8,128)(2,1)} async-done(((bf16[256,1280]{1,0:T(8,128)(2,1)}), bf16[2048,1280]{1,0:T(8,128)(2,1)}) %all-gather.27.cloned.1.call-update) | async-done | bytes 5242896 | tf_op jit(solution)/shard_map/all_gather | solution.py:32
  707.2 86.9 %all-gather.29.cloned.1.call-done = bf16[1280,2048]{1,0:T(8,128)(2,1)} async-done(((bf16[1280,256]{1,0:T(8,128)(2,1)}), bf16[1280,2048]{1,0:T(8,128)(2,1)}) %all-gather.29.cloned.1.call-update) | async-done | bytes 5242896 | tf_op jit(solution)/shard_map/all_gather | solution.py:52
  794.1 16.2 %convolution_convert_fusion.1 = bf16[768,2048]{1,0:T(8,128)(2,1)} fusion(bf16[1280,2048]{1,0:T(8,128)(2,1)} %all-gather.29.cloned.1.call-done, bf16[2048,1280]{1,0:T(8,128)(2,1)} %all-gather.27.cloned.1.call-done, f32[768,1280]{1,0:T(8,128)} %fusion.34, bf16[768,2048]{1,0:T(8,128)(2,1)} %get-tuple-element.7, f32[2048]{0:T(1024)S(1)} %copy-done.5, ...), kind=kOutput, calls=%fused_computation.44 | convolution fusion | flops 8066826240 | bytes 20720640 | tf_op jit(solution)/shard_map/dot_general | solution.py:51
  810.3 0.0 reduce-scatter.8.cloned.1.call-update
  810.4 36.1 %reduce-scatter.8.cloned.1.call-done = bf16[768,512]{1,0:T(8,128)(2,1)} async-done(((bf16[768,2048]{1,0:T(8,128)(2,1)}), bf16[768,512]{1,0:T(8,128)(2,1)}) %reduce-scatter.8.cloned.1.call-update) | async-done | bytes 786448 | tf_op jit(solution)/shard_map/reduce_scatter | solution.py:54
  846.4 2.2 add_convert_fusion
  (23 shorter events, 0.1 us)
Async XLA Ops:
  6.5 91.6 %copy-start.3 = (f32[2048]{0:T(1024)S(1)}, f32[2048]{0:T(1024)}, u32[]{:S(2)}) copy-start(f32[2048]{0:T(1024)} %param.18) | copy-start | bytes 24580
  6.5 91.6 %all-gather.11.cloned.1.call-start = ((), (), s32[]{:S(2)}) async-start(), calls=%async_computation.3 | async-start | bytes 5898240 | tf_op jit(solution)/shard_map/all_gather | solution.py:31
  7.3 177.2 %all-gather.13.cloned.1.call-start = ((), (), s32[]{:S(2)}) async-start(), calls=%async_computation.4 | async-start | bytes 5898240 | tf_op jit(solution)/shard_map/all_gather | solution.py:32
  8.0 263.5 %all-gather.15.cloned.1.call-start = ((), (), s32[]{:S(2)}) async-start(), calls=%async_computation.5 | async-start | bytes 5898240 | tf_op jit(solution)/shard_map/all_gather | solution.py:52
  8.7 315.2 %reduce-scatter.4.cloned.1.call-start = ((), (), s32[]{:S(2)}) async-start(), calls=%async_computation.6 | async-start | bytes 3932160 | tf_op jit(solution)/shard_map/reduce_scatter | solution.py:54
  8.8 12.4 %collective-permute-start = (bf16[768,512]{1,0:T(8,128)(2,1)}, bf16[768,512]{1,0:T(8,128)(2,1)S(1)}, u32[]{:S(2)}, u32[]{:S(2)}) collective-permute-start(bf16[768,512]{1,0:T(8,128)(2,1)} %bitcast.18), channel_id=1, source_target_pairs={{0,1},{1,2},{2,3},{3,0},{4,5},{5,6},{6,7},{7,4},{8,9},{9,10},{10,1... | collective-permute-start | bytes 2359304 | tf_op jit(solution)/shard_map/ppermute | solution.py:12
  21.2 0.9 copy-start
  22.0 11.4 %collective-permute-start.1 = (bf16[768,512]{1,0:T(8,128)(2,1)S(1)}, bf16[768,512]{1,0:T(8,128)(2,1)S(1)}, u32[]{:S(2)}, u32[]{:S(2)}) collective-permute-start(bf16[768,512]{1,0:T(8,128)(2,1)S(1)} %collective-permute-done), channel_id=1, source_target_pairs={{0,1},{1,2},{2,3},{3,0},{4,5},{5,6},{6,7},{7,4},{8,9},{9,10},{10,1... | collective-permute-start | bytes 2359304 | tf_op jit(solution)/shard_map/ppermute | solution.py:12
  33.5 0.9 copy-start.1
  33.5 11.5 %collective-permute-start.2 = (bf16[768,512]{1,0:T(8,128)(2,1)S(1)}, bf16[768,512]{1,0:T(8,128)(2,1)}, u32[]{:S(2)}, u32[]{:S(2)}) collective-permute-start(bf16[768,512]{1,0:T(8,128)(2,1)S(1)} %collective-permute-done.1), channel_id=1, source_target_pairs={{0,1},{1,2},{2,3},{3,0},{4,5},{5,6},{6,7},{7,4},{8,9},{9,10},{10,1... | collective-permute-start | bytes 2359304 | tf_op jit(solution)/shard_map/ppermute | solution.py:12
  287.9 60.6 %copy-start.2 = (f32[3,256]{1,0:T(4,128)S(1)}, f32[3,256]{1,0:T(4,128)}, u32[]{:S(2)}) copy-start(f32[3,256]{1,0:T(4,128)} %param.26) | copy-start | bytes 9220
  287.9 81.5 %copy-start.4 = (f32[2048]{0:T(1024)S(1)}, f32[2048]{0:T(1024)}, u32[]{:S(2)}) copy-start(f32[2048]{0:T(1024)} %param.22) | copy-start | bytes 24580
  287.9 81.5 %all-gather.21.cloned.1.call-start = ((), (), s32[]{:S(2)}) async-start(), calls=%async_computation.9 | async-start | bytes 1179648 | tf_op jit(solution)/shard_map/all_gather | solution.py:43
  288.5 118.7 %all-gather.19.cloned.1.call-start = ((), (), s32[]{:S(2)}) async-start(), calls=%async_computation.8 | async-start | bytes 1179648 | tf_op jit(solution)/shard_map/all_gather | solution.py:46
  289.1 159.3 %all-gather.17.cloned.1.call-start = ((), (), s32[]{:S(2)}) async-start(), calls=%async_computation.7 | async-start | bytes 1179648 | tf_op jit(solution)/shard_map/all_gather | solution.py:45
  325.6 11.5 %collective-permute-start.3 = (bf16[768,512]{1,0:T(8,128)(2,1)S(1)}, bf16[768,512]{1,0:T(8,128)(2,1)S(1)}, u32[]{:S(2)}, u32[]{:S(2)}) collective-permute-start(bf16[768,512]{1,0:T(8,128)(2,1)S(1)} %add_convert_fusion.2), channel_id=1, source_target_pairs={{0,1},{1,2},{2,3},{3,0},{4,5},{5,6},{6,7},{7,4},{8,9},{9,10},{10,1... | collective-permute-start | bytes 2359304 | tf_op jit(solution)/shard_map/ppermute | solution.py:12
  325.6 162.9 %all-gather.23.cloned.1.call-start = ((), (), s32[]{:S(2)}) async-start(), calls=%async_computation.10 | async-start | bytes 1179648 | tf_op jit(solution)/shard_map/all_gather | solution.py:52
  337.0 11.4 %collective-permute-start.4 = (bf16[768,512]{1,0:T(8,128)(2,1)S(1)}, bf16[768,512]{1,0:T(8,128)(2,1)S(1)}, u32[]{:S(2)}, u32[]{:S(2)}) collective-permute-start(bf16[768,512]{1,0:T(8,128)(2,1)S(1)} %collective-permute-done.3), channel_id=1, source_target_pairs={{0,1},{1,2},{2,3},{3,0},{4,5},{5,6},{6,7},{7,4},{8,9},{9,10},{10,1... | collective-permute-start | bytes 2359304 | tf_op jit(solution)/shard_map/ppermute | solution.py:12
  348.4 11.4 %collective-permute-start.5 = (bf16[768,512]{1,0:T(8,128)(2,1)S(1)}, bf16[768,512]{1,0:T(8,128)(2,1)S(1)}, u32[]{:S(2)}, u32[]{:S(2)}) collective-permute-start(bf16[768,512]{1,0:T(8,128)(2,1)S(1)} %collective-permute-done.4), channel_id=1, source_target_pairs={{0,1},{1,2},{2,3},{3,0},{4,5},{5,6},{6,7},{7,4},{8,9},{9,10},{10,1... | collective-permute-start | bytes 2359304 | tf_op jit(solution)/shard_map/ppermute | solution.py:12
  348.5 184.5 %reduce-scatter.6.cloned.1.call-start = ((), (), s32[]{:S(2)}) async-start(), calls=%async_computation.11 | async-start | bytes 3932160 | tf_op jit(solution)/shard_map/reduce_scatter | solution.py:54
  496.1 124.8 %copy-start.5 = (f32[2048]{0:T(1024)S(1)}, f32[2048]{0:T(1024)}, u32[]{:S(2)}) copy-start(f32[2048]{0:T(1024)} %param.28) | copy-start | bytes 24580
  496.1 124.8 %all-gather.25.cloned.1.call-start = ((), (), s32[]{:S(2)}) async-start(), calls=%async_computation.12 | async-start | bytes 5898240 | tf_op jit(solution)/shard_map/all_gather | solution.py:31
  496.7 210.5 %all-gather.27.cloned.1.call-start = ((), (), s32[]{:S(2)}) async-start(), calls=%async_computation.13 | async-start | bytes 5898240 | tf_op jit(solution)/shard_map/all_gather | solution.py:32
  497.4 296.7 %all-gather.29.cloned.1.call-start = ((), (), s32[]{:S(2)}) async-start(), calls=%async_computation.14 | async-start | bytes 5898240 | tf_op jit(solution)/shard_map/all_gather | solution.py:52
  498.0 348.4 %reduce-scatter.8.cloned.1.call-start = ((), (), s32[]{:S(2)}) async-start(), calls=%async_computation.15 | async-start | bytes 3932160 | tf_op jit(solution)/shard_map/reduce_scatter | solution.py:54
  534.3 11.5 %collective-permute-start.6 = (bf16[768,512]{1,0:T(8,128)(2,1)S(1)}, bf16[768,512]{1,0:T(8,128)(2,1)S(1)}, u32[]{:S(2)}, u32[]{:S(2)}) collective-permute-start(bf16[768,512]{1,0:T(8,128)(2,1)S(1)} %add_convert_fusion.1), channel_id=1, source_target_pairs={{0,1},{1,2},{2,3},{3,0},{4,5},{5,6},{6,7},{7,4},{8,9},{9,10},{10,1... | collective-permute-start | bytes 2359304 | tf_op jit(solution)/shard_map/ppermute | solution.py:12
  545.8 11.4 %collective-permute-start.7 = (bf16[768,512]{1,0:T(8,128)(2,1)S(1)}, bf16[768,512]{1,0:T(8,128)(2,1)S(1)}, u32[]{:S(2)}, u32[]{:S(2)}) collective-permute-start(bf16[768,512]{1,0:T(8,128)(2,1)S(1)} %collective-permute-done.6), channel_id=1, source_target_pairs={{0,1},{1,2},{2,3},{3,0},{4,5},{5,6},{6,7},{7,4},{8,9},{9,10},{10,1... | collective-permute-start | bytes 2359304 | tf_op jit(solution)/shard_map/ppermute | solution.py:12
  557.2 11.4 %collective-permute-start.8 = (bf16[768,512]{1,0:T(8,128)(2,1)S(1)}, bf16[768,512]{1,0:T(8,128)(2,1)S(1)}, u32[]{:S(2)}, u32[]{:S(2)}) collective-permute-start(bf16[768,512]{1,0:T(8,128)(2,1)S(1)} %collective-permute-done.7), channel_id=1, source_target_pairs={{0,1},{1,2},{2,3},{3,0},{4,5},{5,6},{6,7},{7,4},{8,9},{9,10},{10,1... | collective-permute-start | bytes 2359304 | tf_op jit(solution)/shard_map/ppermute | solution.py:12
Sparse Core Ops, SparseCore 0:
  9.5 88.5 all-gather.10
  100.3 84.0 all-gather.12
  186.5 84.9 all-gather.14
  288.0 35.8 reduce-scatter.3
  325.9 40.2 all-gather.20
  368.2 38.9 all-gather.18
  409.4 38.9 all-gather.16
  450.4 38.0 all-gather.22
  496.2 36.7 reduce-scatter.5
  535.0 85.8 all-gather.24
  623.1 84.0 all-gather.26
  709.1 84.9 all-gather.28
  810.5 35.8 reduce-scatter.7
